TPU v7x, 32 devices: a whole 2x2x4 slice. The times are simulated.
32 devices in a mesh: rep: 2 (over x), fs: 4 (over z), tp: 4 (over y, core).
Axes of the slice: x: 2, y: 2, z: 4, core: 2. Of those that a mesh axis runs over, the one named last changes fastest.
Arguments:
- tokens: bfloat16 [4096, 2048], P(('rep', 'fs', 'tp')), may hold values from -6 to 6
- mix_gain: bfloat16 [2048], replicated, may hold values from 0.099609375 to 1.8984375
- gate_proj: bfloat16 [2048, 512], P('fs', 'tp'), may hold values from -0.125 to 0.125
- value_proj: bfloat16 [2048, 512], P('fs', 'tp'), may hold values from -1 to 1
- layer_gain: bfloat16 [512], replicated, may hold values from 0.099609375 to 1.8984375
- layer_shift: bfloat16 [512], replicated, may hold values from -3 to 3
- mix_kernel: bfloat16 [4, 128, 128], replicated, may hold values from -0.5 to 0.5
- mix_offset: bfloat16 [4, 128], replicated, may hold values from -4 to 4
- out_proj: bfloat16 [2048, 512], P('fs', 'tp'), may hold values from -0.25 to 0.25
- ffn_gain: bfloat16 [2048], replicated, may hold values from 0.099609375 to 1.8984375
- ffn_gate: bfloat16 [2048, 5632], P('fs', 'tp'), may hold values from -0.125 to 0.125
- ffn_up: bfloat16 [2048, 5632], P('fs', 'tp'), may hold values from -0.125 to 0.125
- ffn_down: bfloat16 [2048, 5632], P('fs', 'tp'), may hold values from -0.078125 to 0.078125
Outputs:
- layer_out: bfloat16 [4096, 2048], P(('rep', 'fs', 'tp'))
All inputs are finite; a program needn't handle non-finite values.
Results may differ from a plain program's by a relative error of at most 0.015.
Values may be sent and summed in bfloat16 or wider, within the bound.
A program may use at most 64 MiB of HBM per device.

v0:
```python
import jax
import jax.numpy as jnp
from jax import lax
from jax.sharding import PartitionSpec as P

epsilon = 1e-06


def rms_norm(rows, gain):
    floats = rows.astype(jnp.float32)
    scale = lax.rsqrt(jnp.mean(floats * floats, axis=-1, keepdims=True) + epsilon)
    return (floats * scale * gain.astype(jnp.float32)).astype(jnp.bfloat16)


def contract_last(left, right):
    return lax.dot_general(
        left, right, (((1,), (1,)), ((), ())), preferred_element_type=jnp.float32
    )


def per_device(
    tokens,
    mix_gain,
    gate_proj,
    value_proj,
    layer_gain,
    layer_shift,
    mix_kernel,
    mix_offset,
    out_proj,
    ffn_gain,
    ffn_gate,
    ffn_up,
    ffn_down,
):
    normed = rms_norm(tokens, mix_gain)
    gate_rows, value_rows, out_rows = (
        lax.all_gather(gate_proj, "fs", axis=0, tiled=True),
        lax.all_gather(value_proj, "fs", axis=0, tiled=True),
        lax.all_gather(out_proj, "fs", axis=0, tiled=True),
    )
    mix_width = layer_gain.shape[0]
    groups = mix_kernel.shape[0]
    span_len = mix_kernel.shape[1]
    causal = jnp.tril(jnp.ones((span_len, span_len), dtype=bool))
    masked = jnp.where(causal[None], mix_kernel, jnp.zeros_like(mix_kernel))
    local_width = gate_rows.shape[1]
    first_col = lax.axis_index("tp") * local_width
    joined = jnp.concatenate([gate_rows, value_rows], axis=1)
    preact = jnp.dot(
        lax.all_gather(normed, "tp", axis=0, tiled=True), joined, preferred_element_type=jnp.float32
    )
    gate_u = jax.nn.gelu(preact[:, :local_width])
    activated = jax.nn.gelu(preact[:, local_width:])
    row_sum, squares = lax.psum(
        (jnp.sum(activated, axis=-1), jnp.sum(activated * activated, axis=-1)), "tp"
    )
    center = (row_sum / mix_width)[:, None]
    spread = (squares / mix_width)[:, None] - center * center
    gain_part = lax.dynamic_slice_in_dim(layer_gain, first_col, local_width).astype(jnp.float32)
    shift_part = lax.dynamic_slice_in_dim(layer_shift, first_col, local_width).astype(jnp.float32)
    values = ((activated - center) * lax.rsqrt(spread + epsilon) * gain_part + shift_part).astype(
        jnp.bfloat16
    )
    group_id = first_col // (mix_width // groups)
    kernel = lax.dynamic_index_in_dim(masked, group_id, 0, keepdims=False)
    offset = lax.dynamic_index_in_dim(mix_offset, group_id, 0, keepdims=False).astype(jnp.float32)
    mixing = jnp.einsum(
        "ts,nsc->ntc",
        kernel,
        values.reshape(-1, span_len, local_width),
        preferred_element_type=jnp.float32,
    )
    mixing = mixing + offset[None, :, None]
    gated_rows = (gate_u * mixing.reshape(gate_u.shape)).astype(jnp.bfloat16)
    mixer_out = lax.psum_scatter(
        contract_last(gated_rows, out_rows).astype(jnp.bfloat16),
        "tp",
        scatter_dimension=0,
        tiled=True,
    ).astype(jnp.float32)
    middle = (tokens.astype(jnp.float32) + mixer_out).astype(jnp.bfloat16)
    normed2 = rms_norm(middle, ffn_gain)
    gathered = lax.all_gather(normed2, "tp", axis=0, tiled=True)
    gate_pre = jnp.dot(
        gathered,
        lax.all_gather(ffn_gate, "fs", axis=0, tiled=True),
        preferred_element_type=jnp.float32,
    )
    up_pre = jnp.dot(
        gathered,
        lax.all_gather(ffn_up, "fs", axis=0, tiled=True),
        preferred_element_type=jnp.float32,
    )
    hidden = (jax.nn.silu(gate_pre) * up_pre).astype(jnp.bfloat16)
    partial_value = contract_last(hidden, lax.all_gather(ffn_down, "fs", axis=0, tiled=True))
    summed = lax.psum_scatter(
        partial_value.astype(jnp.bfloat16), "tp", scatter_dimension=0, tiled=True
    ).astype(jnp.float32)
    return (middle.astype(jnp.float32) + summed).astype(jnp.bfloat16)


def solution(mesh):
    placed = (
        P(("rep", "fs", "tp"), None),
        P(),
        P("fs", "tp"),
        P("fs", "tp"),
        P(),
        P(),
        P(),
        P(),
        P("fs", "tp"),
        P(),
        P("fs", "tp"),
        P("fs", "tp"),
        P("fs", "tp"),
    )
    return jax.shard_map(
        per_device,
        mesh=mesh,
        in_specs=placed,
        out_specs=P(("rep", "fs", "tp"), None),
        check_vma=False,
    )
```

profile of v0, /device:TPU:0, one launch (start us, length us, event | category | flops | bytes accessed | tf_op | source)
XLA Modules:
  0.0 472.7 jit_solution(3375747574779029369)
XLA Ops:
  7.4 0.0 copy-start.2
  7.4 0.0 copy-start.3
  7.4 0.0 all-gather.6.cloned.1.call-start
  7.4 0.7 convert_element_type.64
  8.1 1.2 fusion.1
  9.3 2.0 fusion.3
  11.4 0.0 all-gather.6.cloned.1.call-update
  11.4 0.0 reduce-scatter.3.cloned.1.call-start
  11.5 0.7 bitcast_convert_fusion
  12.2 0.8 dynamic-slice_convert_fusion
  12.9 17.6 %all_gather.25 = bf16[2048,128]{1,0:T(8,128)(2,1)S(1)} all-gather(bf16[512,128]{1,0:T(8,128)(2,1)} %param.15), channel_id=1, replica_groups=mesh['rep'=2,'fs'=4,'tp'=4] {'fs'}, dimensions={0}, use_global_device_ids=true | all-gather | bytes 655360 | tf_op jit(solution)/shard_map/all_gather | solution.py:38
  30.5 0.0 copy-done.2
  30.5 16.7 %all_gather.26 = bf16[2048,128]{1,0:T(8,128)(2,1)S(1)} all-gather(bf16[512,128]{1,0:T(8,128)(2,1)S(1)} %copy-done.2), channel_id=1, replica_groups=mesh['rep'=2,'fs'=4,'tp'=4] {'fs'}, dimensions={0}, use_global_device_ids=true | all-gather | bytes 655360 | tf_op jit(solution)/shard_map/all_gather | solution.py:39
  47.2 0.0 copy-done.3
  47.2 15.6 %all_gather.27 = bf16[2048,128]{1,0:T(8,128)(2,1)S(1)} all-gather(bf16[512,128]{1,0:T(8,128)(2,1)S(1)} %copy-done.3), channel_id=1, replica_groups=mesh['rep'=2,'fs'=4,'tp'=4] {'fs'}, dimensions={0}, use_global_device_ids=true | all-gather | bytes 655360 | tf_op jit(solution)/shard_map/all_gather | solution.py:40
  62.8 0.0 all-gather.6.cloned.1.call-done
  62.8 2.3 fusion.9
  65.2 0.2 fusion.37
  65.4 5.7 %all-reduce = (f32[512]{0:T(512)S(1)}, f32[512]{0:T(512)S(1)}) all-reduce(f32[512]{0:T(512)S(1)} %get-tuple-element.6, f32[512]{0:T(512)S(1)} %get-tuple-element.5), channel_id=1, replica_groups=mesh['rep'=2,'fs'=4,'tp'=4] {'tp'}, use_global_device_ids=true, to_apply=%region_4.5 | all-reduce | flops 1024 | bytes 8192 | tf_op jit(solution)/shard_map/psum | solution.py:55
  71.1 0.2 add_convert_fusion
  71.3 0.9 convolution_add_fusion
  72.2 0.1 fusion.21
  72.3 0.0 copy-start.4
  72.4 0.0 copy-start
  72.4 2.1 convolution_convert_fusion
  74.4 0.0 reduce-scatter.3.cloned.1.call-update
  74.5 0.0 all-gather.10.cloned.1.call-start
  74.5 0.5 all-gather.10.cloned.1.call-update
  75.0 0.0 all-gather.8.cloned.1.call-start
  75.1 0.0 copy-done.4
  75.1 31.4 %reduce-scatter.3.cloned.1.call-done = bf16[128,2048]{1,0:T(8,128)(2,1)} async-done(((bf16[512,2048]{1,0:T(8,128)(2,1)}), bf16[128,2048]{1,0:T(8,128)(2,1)}) %reduce-scatter.3.cloned.1.call-update) | async-done | bytes 524304 | tf_op jit(solution)/shard_map/reduce_scatter | solution.py:76
  106.5 0.0 copy-done
  106.5 1.3 fusion.5
  107.8 2.0 fusion.7
  109.9 0.0 all-gather.8.cloned.1.call-update
  109.9 0.0 all-gather.12.cloned.1.call-start
  110.0 0.5 all-gather.12.cloned.1.call-update
  110.5 0.0 all-gather.14.cloned.1.call-start
  110.6 0.7 all-gather.14.cloned.1.call-update
  111.2 0.0 reduce-scatter.5.cloned.1.call-start
  111.3 72.6 %all-gather.10.cloned.1.call-done = bf16[2048,1408]{1,0:T(8,128)(2,1)} async-done(((bf16[512,1408]{1,0:T(8,128)(2,1)}), bf16[2048,1408]{1,0:T(8,128)(2,1)}) %all-gather.10.cloned.1.call-update) | async-done | bytes 5767184 | tf_op jit(solution)/shard_map/all_gather | solution.py:87
  183.9 22.1 %all-gather.8.cloned.1.call-done = bf16[512,2048]{1,0:T(8,128)(2,1)} async-done(((bf16[128,2048]{1,0:T(8,128)(2,1)}), bf16[512,2048]{1,0:T(8,128)(2,1)}) %all-gather.8.cloned.1.call-update) | async-done | bytes 2097168 | tf_op jit(solution)/shard_map/all_gather | solution.py:84
  206.0 0.0 copy-start.5
  206.0 8.4 %fusion.38 = f32[512,1408]{1,0:T(8,128)} fusion(bf16[512,2048]{1,0:T(8,128)(2,1)} %all-gather.8.cloned.1.call-done, bf16[2048,1408]{1,0:T(8,128)(2,1)} %all-gather.10.cloned.1.call-done), kind=kOutput, calls=%fused_computation.60 | convolution fusion | flops 2952790016 | bytes 10747904 | tf_op jit(solution)/shard_map/dot_general | solution.py:85
  214.4 0.0 copy-start.1
  214.4 99.6 %all-gather.12.cloned.1.call-done = bf16[2048,1408]{1,0:T(8,128)(2,1)} async-done(((bf16[512,1408]{1,0:T(8,128)(2,1)}), bf16[2048,1408]{1,0:T(8,128)(2,1)}) %all-gather.12.cloned.1.call-update) | async-done | bytes 5767184 | tf_op jit(solution)/shard_map/all_gather | solution.py:92
  314.0 106.4 %all-gather.14.cloned.1.call-done = bf16[2048,1408]{1,0:T(8,128)(2,1)} async-done(((bf16[512,1408]{1,0:T(8,128)(2,1)}), bf16[2048,1408]{1,0:T(8,128)(2,1)}) %all-gather.14.cloned.1.call-update) | async-done | bytes 5767184 | tf_op jit(solution)/shard_map/all_gather | solution.py:96
  420.5 0.0 copy-done.5
  420.5 13.2 %convolution_convert_fusion.1 = bf16[512,2048]{1,0:T(8,128)(2,1)} fusion(bf16[2048,1408]{1,0:T(8,128)(2,1)} %all-gather.14.cloned.1.call-done, bf16[512,2048]{1,0:T(8,128)(2,1)S(1)} %copy-done.5, bf16[2048,1408]{1,0:T(8,128)(2,1)} %all-gather.12.cloned.1.call-done, f32[512,1408]{1,0:T(8,128)} %fusion.38), kind=kOutput, calls=%fused_computation.3 | convolution fusion | flops 5910953984 | bytes 18612224 | tf_op jit(solution)/shard_map/dot_general | solution.py:16
  433.7 0.0 reduce-scatter.5.cloned.1.call-update
  433.7 29.6 %reduce-scatter.5.cloned.1.call-done = bf16[128,2048]{1,0:T(8,128)(2,1)} async-done(((bf16[512,2048]{1,0:T(8,128)(2,1)}), bf16[128,2048]{1,0:T(8,128)(2,1)}) %reduce-scatter.5.cloned.1.call-update) | async-done | bytes 524304 | tf_op jit(solution)/shard_map/reduce_scatter | solution.py:97
  463.3 0.0 copy-done.1
  463.3 2.1 fusion.8
  (5 shorter events, 0.0 us)
Async XLA Ops:
  7.4 23.2 %copy-start.2 = (bf16[512,128]{1,0:T(8,128)(2,1)S(1)}, bf16[512,128]{1,0:T(8,128)(2,1)}, u32[]{:S(2)}) copy-start(bf16[512,128]{1,0:T(8,128)(2,1)} %param.16) | copy-start | bytes 393220
  7.4 39.9 %copy-start.3 = (bf16[512,128]{1,0:T(8,128)(2,1)S(1)}, bf16[512,128]{1,0:T(8,128)(2,1)}, u32[]{:S(2)}) copy-start(bf16[512,128]{1,0:T(8,128)(2,1)} %param.21) | copy-start | bytes 393220
  7.4 55.5 %all-gather.6.cloned.1.call-start = ((), (), s32[]{:S(2)}) async-start(), calls=%async_computation.2 | async-start | bytes 2621440 | tf_op jit(solution)/shard_map/all_gather | solution.py:51
  11.4 95.1 %reduce-scatter.3.cloned.1.call-start = ((), (), s32[]{:S(2)}) async-start(), calls=%async_computation.3 | async-start | bytes 2621440 | tf_op jit(solution)/shard_map/reduce_scatter | solution.py:76
  72.3 2.7 copy-start.4
  72.4 34.2 %copy-start = (bf16[128,2048]{1,0:T(8,128)(2,1)S(1)}, bf16[128,2048]{1,0:T(8,128)(2,1)}, u32[]{:S(2)}) copy-start(bf16[128,2048]{1,0:T(8,128)(2,1)} %param.13) | copy-start | bytes 1572868
  74.5 109.4 %all-gather.10.cloned.1.call-start = ((), (), s32[]{:S(2)}) async-start(), calls=%async_computation.5 | async-start | bytes 7208960 | tf_op jit(solution)/shard_map/all_gather | solution.py:87
  75.0 131.0 %all-gather.8.cloned.1.call-start = ((), (), s32[]{:S(2)}) async-start(), calls=%async_computation.4 | async-start | bytes 2621440 | tf_op jit(solution)/shard_map/all_gather | solution.py:84
  109.9 204.1 %all-gather.12.cloned.1.call-start = ((), (), s32[]{:S(2)}) async-start(), calls=%async_computation.6 | async-start | bytes 7208960 | tf_op jit(solution)/shard_map/all_gather | solution.py:92
  110.5 310.0 %all-gather.14.cloned.1.call-start = ((), (), s32[]{:S(2)}) async-start(), calls=%async_computation.7 | async-start | bytes 7208960 | tf_op jit(solution)/shard_map/all_gather | solution.py:96
  111.2 352.1 %reduce-scatter.5.cloned.1.call-start = ((), (), s32[]{:S(2)}) async-start(), calls=%async_computation.8 | async-start | bytes 2621440 | tf_op jit(solution)/shard_map/reduce_scatter | solution.py:97
  206.0 214.5 %copy-start.5 = (bf16[512,2048]{1,0:T(8,128)(2,1)S(1)}, bf16[512,2048]{1,0:T(8,128)(2,1)}, u32[]{:S(2)}) copy-start(bf16[512,2048]{1,0:T(8,128)(2,1)} %all-gather.8.cloned.1.call-done) | copy-start | bytes 6291460
  214.4 248.9 %copy-start.1 = (bf16[128,2048]{1,0:T(8,128)(2,1)S(1)}, bf16[128,2048]{1,0:T(8,128)(2,1)}, u32[]{:S(2)}) copy-start(bf16[128,2048]{1,0:T(8,128)(2,1)} %reduce-scatter.3.cloned.1.call-done) | copy-start | bytes 1572868
Sparse Core Ops, SparseCore 0:
  11.5 25.2 all-gather.5
  74.6 31.9 reduce-scatter.2
  433.8 29.4 reduce-scatter.4
Sparse Core Ops, SparseCore 1:
  76.5 107.3 all-gather.9
  185.3 20.7 all-gather.7
  207.5 106.5 all-gather.11
  315.6 104.8 all-gather.13
where the time goes:
time: 473 us
  waiting for transfers between devices  364 us (77%)
  blocking collectives  55.5 us (12%)
  matrix products  26.9 us (6%)
  between operations  14.9 us (3%)
  other arithmetic  11.5 us (2%)
    all_gather x1, waiting for transfers between devices, per_device(): lax.all_gather(ffn_down, 'fs', axis=0, tiled=True)  106 us
    all_gather x1, waiting for transfers between devices, per_device(): lax.all_gather(ffn_up, 'fs', axis=0, tiled=True)  99.6 us
    all_gather x1, waiting for transfers between devices, per_device(): lax.all_gather(ffn_gate, 'fs', axis=0, tiled=True)  72.6 us
    reduce_scatter x1, waiting for transfers between devices, per_device(): lax.psum_scatter(contract_last(gated_rows, out_rows).astype(jnp.bfloat16)...  31.4 us
    reduce_scatter x1, waiting for transfers between devices, per_device(): lax.psum_scatter(partial_value.astype(jnp.bfloat16), 'tp', scatter_dimens...  29.6 us
    all_gather x1, waiting for transfers between devices, per_device(): gathered = lax.all_gather(normed2, 'tp', axis=0, tiled=True)  22.1 us
    all_gather x1, blocking collectives, per_device(): lax.all_gather(gate_proj, 'fs', axis=0, tiled=True)  17.6 us
    all_gather x1, blocking collectives, per_device(): lax.all_gather(value_proj, 'fs', axis=0, tiled=True)  16.7 us
  transfers between devices with their start and end apart: 7, of which 6 were waited for; matrix products, arithmetic and copies ran while one was open for 3% of the time, Pallas kernels for 0%

commit v1 on v0

--- a/solution.py
+++ b/solution.py
@@ -4,6 +4,23 @@
 from jax.sharding import PartitionSpec as P
 
 epsilon = 1e-06
+
+
+def detail_the_sectors(sample, where_dim=0):
+    wide_n = lax.axis_size("fs")
+    seen = [(j, (j + 1) % wide_n) for j in range(wide_n)]
+    chunks = [(j, (j - 1) % wide_n) for j in range(wide_n)]
+    all_rows, outer = ([sample], [sample])
+    for _ in range(wide_n // 2):
+        e_next = lax.ppermute(all_rows[-1], "fs", seen)
+        all_rows.append(e_next)
+    for _ in range((wide_n - 1) // 2):
+        arr_next = lax.ppermute(outer[-1], "fs", chunks)
+        outer.append(arr_next)
+    vec_out = jnp.concatenate([*all_rows[::-1], *outer[1:]], where_dim)
+    return jnp.roll(
+        vec_out, (lax.axis_index("fs") - wide_n // 2) * sample.shape[where_dim], where_dim
+    )
 
 
 def rms_norm(rows, gain):
@@ -87,11 +104,7 @@
         lax.all_gather(ffn_gate, "fs", axis=0, tiled=True),
         preferred_element_type=jnp.float32,
     )
-    up_pre = jnp.dot(
-        gathered,
-        lax.all_gather(ffn_up, "fs", axis=0, tiled=True),
-        preferred_element_type=jnp.float32,
-    )
+    up_pre = jnp.dot(gathered, detail_the_sectors(ffn_up), preferred_element_type=jnp.float32)
     hidden = (jax.nn.silu(gate_pre) * up_pre).astype(jnp.bfloat16)
     partial_value = contract_last(hidden, lax.all_gather(ffn_down, "fs", axis=0, tiled=True))
     summed = lax.psum_scatter(

time: 473 us -> 432 us (0.913)
  waiting for transfers between devices: 364 us -> 272 us
  starting transfers between devices: 0.26 us -> 34.9 us
  local copies, waits for them, and re-layouts: 0.03 us -> 15.6 us
    ppermute x0 -> x3, waiting for transfers between devices: none -> 124 us  [the longest x2 101 us: detail_the_sectors(): e_next = lax.ppermute(all_rows[-1], 'fs', seen)]
    all_gather x1 -> x0, waiting for transfers between devices: 99.6 us -> none  [per_device(): lax.all_gather(ffn_up, 'fs', axis=0, tiled=True)]
    all_gather x1, waiting for transfers between devices: 72.6 us -> 0.01 us  [per_device(): lax.all_gather(ffn_gate, 'fs', axis=0, tiled=True)]
    ppermute x0 -> x3, starting transfers between devices: none -> 34.6 us  [the longest x2 28.4 us: detail_the_sectors(): e_next = lax.ppermute(all_rows[-1], 'fs', seen)]
    all_gather x1, waiting for transfers between devices: 22.1 us -> 0.01 us  [per_device(): gathered = lax.all_gather(normed2, 'tp', axis=0, tiled=True)]
    all_gather x1, waiting for transfers between devices: 106 us -> 86.2 us  [per_device(): lax.all_gather(ffn_down, 'fs', axis=0, tiled=True)]
    unnamed x12 -> x21, local copies, waits for them, and re-layouts: 0.03 us -> 12.9 us
  transfers between devices with their start and end apart: 7 -> 9, of which waited for: 6 -> 6; matrix products, arithmetic and copies ran while one was open for 3% -> 7% of each run, Pallas kernels for 0% -> 0%
where the time goes in v1:
time: 432 us
  waiting for transfers between devices  272 us (63%)
  blocking collectives  55.5 us (13%)
  starting transfers between devices  34.9 us (8%)
  matrix products  27 us (6%)
  local copies, waits for them, and re-layouts  15.6 us (4%)
  between operations  14.9 us (3%)
  other arithmetic  11.5 us (3%)
    ppermute x2, waiting for transfers between devices, detail_the_sectors(): e_next = lax.ppermute(all_rows[-1], 'fs', seen)  101 us
    all_gather x1, waiting for transfers between devices, per_device(): lax.all_gather(ffn_down, 'fs', axis=0, tiled=True)  86.2 us
    reduce_scatter x1, waiting for transfers between devices, per_device(): lax.psum_scatter(contract_last(gated_rows, out_rows).astype(jnp.bfloat16)...  31.4 us
    reduce_scatter x1, waiting for transfers between devices, per_device(): lax.psum_scatter(partial_value.astype(jnp.bfloat16), 'tp', scatter_dimens...  29.6 us
    ppermute x2, starting transfers between devices, detail_the_sectors(): e_next = lax.ppermute(all_rows[-1], 'fs', seen)  28.4 us
    ppermute x1, waiting for transfers between devices, detail_the_sectors(): arr_next = lax.ppermute(outer[-1], 'fs', chunks)  23.1 us
    all_gather x1, blocking collectives, per_device(): lax.all_gather(gate_proj, 'fs', axis=0, tiled=True)  17.6 us
    all_gather x1, blocking collectives, per_device(): lax.all_gather(value_proj, 'fs', axis=0, tiled=True)  16.7 us
  transfers between devices with their start and end apart: 9, of which 6 were waited for; matrix products, arithmetic and copies ran while one was open for 7% of the time, Pallas kernels for 0%

profile of v1, /device:TPU:0, one launch (start us, length us, event | category | flops | bytes accessed | tf_op | source)
XLA Modules:
  0.0 431.5 jit_solution(6863769381710729109)
XLA Ops:
  7.4 0.0 copy-start.3
  7.4 0.0 copy-start.4
  7.4 0.0 all-gather.5.cloned.1.call-start
  7.4 0.7 convert_element_type.64
  8.1 1.2 fusion.8
  9.3 2.0 fusion.10
  11.4 0.0 all-gather.5.cloned.1.call-update
  11.4 0.0 reduce-scatter.3.cloned.1.call-start
  11.5 0.7 fusion.46
  12.2 0.8 dynamic-slice_convert_fusion
  12.9 17.6 %all_gather.22 = bf16[2048,128]{1,0:T(8,128)(2,1)S(1)} all-gather(bf16[512,128]{1,0:T(8,128)(2,1)} %param.15), channel_id=1, replica_groups=mesh['rep'=2,'fs'=4,'tp'=4] {'fs'}, dimensions={0}, use_global_device_ids=true | all-gather | bytes 655360 | tf_op jit(solution)/shard_map/all_gather | solution.py:55
  30.5 0.0 copy-done.3
  30.5 16.7 %all_gather.23 = bf16[2048,128]{1,0:T(8,128)(2,1)S(1)} all-gather(bf16[512,128]{1,0:T(8,128)(2,1)S(1)} %copy-done.3), channel_id=1, replica_groups=mesh['rep'=2,'fs'=4,'tp'=4] {'fs'}, dimensions={0}, use_global_device_ids=true | all-gather | bytes 655360 | tf_op jit(solution)/shard_map/all_gather | solution.py:56
  47.2 0.0 copy-done.4
  47.2 15.6 %all_gather.24 = bf16[2048,128]{1,0:T(8,128)(2,1)S(1)} all-gather(bf16[512,128]{1,0:T(8,128)(2,1)S(1)} %copy-done.4), channel_id=1, replica_groups=mesh['rep'=2,'fs'=4,'tp'=4] {'fs'}, dimensions={0}, use_global_device_ids=true | all-gather | bytes 655360 | tf_op jit(solution)/shard_map/all_gather | solution.py:57
  62.8 0.0 all-gather.5.cloned.1.call-done
  62.8 2.3 fusion.16
  65.1 0.2 fusion.50
  65.4 5.7 %all-reduce = (f32[512]{0:T(512)S(1)}, f32[512]{0:T(512)S(1)}) all-reduce(f32[512]{0:T(512)S(1)} %get-tuple-element.6, f32[512]{0:T(512)S(1)} %get-tuple-element.5), channel_id=1, replica_groups=mesh['rep'=2,'fs'=4,'tp'=4] {'tp'}, use_global_device_ids=true, to_apply=%region_4.5 | all-reduce | flops 1024 | bytes 8192 | tf_op jit(solution)/shard_map/psum | solution.py:72
  71.1 0.2 add_convert_fusion
  71.3 0.9 convolution_add_fusion
  72.2 0.1 fusion.30
  72.3 0.0 copy-start.5
  72.3 0.0 copy-start
  72.4 2.0 convolution_convert_fusion
  74.4 0.0 reduce-scatter.3.cloned.1.call-update
  74.4 0.0 copy-start.1
  74.4 0.0 all-gather.9.cloned.1.call-start
  74.5 0.5 all-gather.9.cloned.1.call-update
  75.0 0.0 all-gather.7.cloned.1.call-start
  75.1 0.0 copy-done.5
  75.1 31.4 %reduce-scatter.3.cloned.1.call-done = bf16[128,2048]{1,0:T(8,128)(2,1)} async-done(((bf16[512,2048]{1,0:T(8,128)(2,1)}), bf16[128,2048]{1,0:T(8,128)(2,1)}) %reduce-scatter.3.cloned.1.call-update) | async-done | bytes 524304 | tf_op jit(solution)/shard_map/reduce_scatter | solution.py:93
  106.5 0.0 copy-done
  106.5 1.3 fusion.12
  107.8 2.0 fusion.14
  109.9 0.0 all-gather.7.cloned.1.call-update
  109.9 0.0 all-gather.11.cloned.1.call-start
  109.9 0.5 all-gather.11.cloned.1.call-update
  110.5 0.0 reduce-scatter.5.cloned.1.call-start
  110.5 0.0 copy-done.1
  110.5 1.5 collective-permute-start
  112.1 65.3 %collective-permute-done = bf16[512,1408]{1,0:T(8,128)(2,1)S(1)} collective-permute-done((bf16[512,1408]{1,0:T(8,128)(2,1)S(1)}, bf16[512,1408]{1,0:T(8,128)(2,1)S(1)}, u32[]{:S(2)}, u32[]{:S(2)}) %collective-permute-start) | collective-permute-done | bytes 1441824 | tf_op jit(solution)/shard_map/ppermute | solution.py:15
  177.4 26.8 %collective-permute-start.1 = (bf16[512,1408]{1,0:T(8,128)(2,1)S(1)}, bf16[512,1408]{1,0:T(8,128)(2,1)}, u32[]{:S(2)}, u32[]{:S(2)}) collective-permute-start(bf16[512,1408]{1,0:T(8,128)(2,1)S(1)} %collective-permute-done), channel_id=1, source_target_pairs={{0,4},{4,8},{8,12},{12,0},{1,5},{5,9},{9,13},{13,1},{2,6},{6,10},{... | collective-permute-start | bytes 4325384 | tf_op jit(solution)/shard_map/ppermute | solution.py:15
  204.2 6.3 %collective-permute-start.2 = (bf16[512,1408]{1,0:T(8,128)(2,1)S(1)}, bf16[512,1408]{1,0:T(8,128)(2,1)}, u32[]{:S(2)}, u32[]{:S(2)}) collective-permute-start(bf16[512,1408]{1,0:T(8,128)(2,1)S(1)} %copy-done.1), channel_id=1, source_target_pairs={{0,12},{4,0},{8,4},{12,8},{1,13},{5,1},{9,5},{13,9},{2,14},{6,2},{... | collective-permute-start | bytes 4325384 | tf_op jit(solution)/shard_map/ppermute | solution.py:18
  210.5 35.5 %collective-permute-done.1 = bf16[512,1408]{1,0:T(8,128)(2,1)} collective-permute-done((bf16[512,1408]{1,0:T(8,128)(2,1)S(1)}, bf16[512,1408]{1,0:T(8,128)(2,1)}, u32[]{:S(2)}, u32[]{:S(2)}) %collective-permute-start.1) | collective-permute-done | bytes 1441824 | tf_op jit(solution)/shard_map/ppermute | solution.py:15
  246.0 2.6 constant_dynamic-update-slice_fusion.7
  248.6 1.2 constant_dynamic-update-slice_fusion.6
  249.8 1.2 constant_dynamic-update-slice_fusion.5
  251.0 23.1 %collective-permute-done.2 = bf16[512,1408]{1,0:T(8,128)(2,1)} collective-permute-done((bf16[512,1408]{1,0:T(8,128)(2,1)S(1)}, bf16[512,1408]{1,0:T(8,128)(2,1)}, u32[]{:S(2)}, u32[]{:S(2)}) %collective-permute-start.2) | collective-permute-done | bytes 1441824 | tf_op jit(solution)/shard_map/ppermute | solution.py:18
  274.1 2.6 constant_dynamic-update-slice_fusion.4
  276.7 2.6 constant_dynamic-update-slice_fusion.3
  279.3 1.3 constant_dynamic-update-slice_fusion.2
  280.6 1.3 constant_dynamic-update-slice_fusion.1
  281.9 2.7 constant_dynamic-update-slice_fusion
  284.6 0.0 all-gather.9.cloned.1.call-done
  284.6 0.0 all-gather.7.cloned.1.call-done
  284.6 8.4 %fusion.51 = f32[512,1408]{1,0:T(8,128)} fusion(bf16[512,2048]{1,0:T(8,128)(2,1)} %all-gather.7.cloned.1.call-done, bf16[2048,1408]{1,0:T(8,128)(2,1)} %all-gather.9.cloned.1.call-done), kind=kOutput, calls=%fused_computation.73 | convolution fusion | flops 2952790016 | bytes 10747904 | tf_op jit(solution)/shard_map/dot_general | solution.py:102
  293.0 86.2 %all-gather.11.cloned.1.call-done = bf16[2048,1408]{1,0:T(8,128)(2,1)} async-done(((bf16[512,1408]{1,0:T(8,128)(2,1)}), bf16[2048,1408]{1,0:T(8,128)(2,1)}) %all-gather.11.cloned.1.call-update) | async-done | bytes 5767184 | tf_op jit(solution)/shard_map/all_gather | solution.py:109
  379.2 0.0 copy-done.6
  379.2 13.3 %convolution_convert_fusion.1 = bf16[512,2048]{1,0:T(8,128)(2,1)} fusion(bf16[2048,1408]{1,0:T(8,128)(2,1)} %all-gather.11.cloned.1.call-done, bf16[512,2048]{1,0:T(8,128)(2,1)S(1)} %copy-done.6, bf16[4096,1408]{1,0:T(8,128)(2,1)} %constant_dynamic-update-slice_fusion, s32[]{:T(128)S(6)} %select_n.38, f32[512,1408]{1,0:T(8,128)} %fusion.51), kind=kOutput, calls=%fused_computation.5 | convolution fusion | flops 5910953984 | bytes 18612228 | tf_op jit(solution)/shard_map/dot_general | solution.py:33
  392.5 0.0 reduce-scatter.5.cloned.1.call-update
  392.5 29.6 %reduce-scatter.5.cloned.1.call-done = bf16[128,2048]{1,0:T(8,128)(2,1)} async-done(((bf16[512,2048]{1,0:T(8,128)(2,1)}), bf16[128,2048]{1,0:T(8,128)(2,1)}) %reduce-scatter.5.cloned.1.call-update) | async-done | bytes 524304 | tf_op jit(solution)/shard_map/reduce_scatter | solution.py:110
  422.1 0.0 copy-done.2
  422.1 2.1 fusion.15
  (7 shorter events, 0.0 us)
Async XLA Ops:
  7.4 23.2 %copy-start.3 = (bf16[512,128]{1,0:T(8,128)(2,1)S(1)}, bf16[512,128]{1,0:T(8,128)(2,1)}, u32[]{:S(2)}) copy-start(bf16[512,128]{1,0:T(8,128)(2,1)} %param.16) | copy-start | bytes 393220
  7.4 39.9 %copy-start.4 = (bf16[512,128]{1,0:T(8,128)(2,1)S(1)}, bf16[512,128]{1,0:T(8,128)(2,1)}, u32[]{:S(2)}) copy-start(bf16[512,128]{1,0:T(8,128)(2,1)} %param.21) | copy-start | bytes 393220
  7.4 55.5 %all-gather.5.cloned.1.call-start = ((), (), s32[]{:S(2)}) async-start(), calls=%async_computation.2 | async-start | bytes 2621440 | tf_op jit(solution)/shard_map/all_gather | solution.py:68
  11.4 95.1 %reduce-scatter.3.cloned.1.call-start = ((), (), s32[]{:S(2)}) async-start(), calls=%async_computation.3 | async-start | bytes 2621440 | tf_op jit(solution)/shard_map/reduce_scatter | solution.py:93
  72.3 2.7 copy-start.5
  72.3 34.2 %copy-start = (bf16[128,2048]{1,0:T(8,128)(2,1)S(1)}, bf16[128,2048]{1,0:T(8,128)(2,1)}, u32[]{:S(2)}) copy-start(bf16[128,2048]{1,0:T(8,128)(2,1)} %param.13) | copy-start | bytes 1572868
  74.4 36.1 %copy-start.1 = (bf16[512,1408]{1,0:T(8,128)(2,1)S(1)}, bf16[512,1408]{1,0:T(8,128)(2,1)}, u32[]{:S(2)}) copy-start(bf16[512,1408]{1,0:T(8,128)(2,1)} %param.24) | copy-start | bytes 4325380
  74.4 210.1 %all-gather.9.cloned.1.call-start = ((), (), s32[]{:S(2)}) async-start(), calls=%async_computation.5 | async-start | bytes 7208960 | tf_op jit(solution)/shard_map/all_gather | solution.py:104
  75.0 209.6 %all-gather.7.cloned.1.call-start = ((), (), s32[]{:S(2)}) async-start(), calls=%async_computation.4 | async-start | bytes 2621440 | tf_op jit(solution)/shard_map/all_gather | solution.py:101
  109.9 269.3 %all-gather.11.cloned.1.call-start = ((), (), s32[]{:S(2)}) async-start(), calls=%async_computation.6 | async-start | bytes 7208960 | tf_op jit(solution)/shard_map/all_gather | solution.py:109
  110.5 311.6 %reduce-scatter.5.cloned.1.call-start = ((), (), s32[]{:S(2)}) async-start(), calls=%async_computation.7 | async-start | bytes 2621440 | tf_op jit(solution)/shard_map/reduce_scatter | solution.py:110
  110.5 66.8 %collective-permute-start = (bf16[512,1408]{1,0:T(8,128)(2,1)S(1)}, bf16[512,1408]{1,0:T(8,128)(2,1)S(1)}, u32[]{:S(2)}, u32[]{:S(2)}) collective-permute-start(bf16[512,1408]{1,0:T(8,128)(2,1)S(1)} %copy-done.1), channel_id=1, source_target_pairs={{0,4},{4,8},{8,12},{12,0},{1,5},{5,9},{9,13},{13,1},{2,6},{6,10},{... | collective-permute-start | bytes 4325384 | tf_op jit(solution)/shard_map/ppermute | solution.py:15
  177.4 68.6 %collective-permute-start.1 = (bf16[512,1408]{1,0:T(8,128)(2,1)S(1)}, bf16[512,1408]{1,0:T(8,128)(2,1)}, u32[]{:S(2)}, u32[]{:S(2)}) collective-permute-start(bf16[512,1408]{1,0:T(8,128)(2,1)S(1)} %collective-permute-done), channel_id=1, source_target_pairs={{0,4},{4,8},{8,12},{12,0},{1,5},{5,9},{9,13},{13,1},{2,6},{6,10},{... | collective-permute-start | bytes 4325384 | tf_op jit(solution)/shard_map/ppermute | solution.py:15
  204.2 69.9 %collective-permute-start.2 = (bf16[512,1408]{1,0:T(8,128)(2,1)S(1)}, bf16[512,1408]{1,0:T(8,128)(2,1)}, u32[]{:S(2)}, u32[]{:S(2)}) collective-permute-start(bf16[512,1408]{1,0:T(8,128)(2,1)S(1)} %copy-done.1), channel_id=1, source_target_pairs={{0,12},{4,0},{8,4},{12,8},{1,13},{5,1},{9,5},{13,9},{2,14},{6,2},{... | collective-permute-start | bytes 4325384 | tf_op jit(solution)/shard_map/ppermute | solution.py:18
  284.6 94.6 %copy-start.6 = (bf16[512,2048]{1,0:T(8,128)(2,1)S(1)}, bf16[512,2048]{1,0:T(8,128)(2,1)}, u32[]{:S(2)}) copy-start(bf16[512,2048]{1,0:T(8,128)(2,1)} %all-gather.7.cloned.1.call-done) | copy-start | bytes 6291460
  293.0 129.1 %copy-start.2 = (bf16[128,2048]{1,0:T(8,128)(2,1)S(1)}, bf16[128,2048]{1,0:T(8,128)(2,1)}, u32[]{:S(2)}) copy-start(bf16[128,2048]{1,0:T(8,128)(2,1)} %reduce-scatter.3.cloned.1.call-done) | copy-start | bytes 1572868
Sparse Core Ops, SparseCore 0:
  11.5 25.2 all-gather.4
  74.5 31.9 reduce-scatter.2
  392.6 29.4 reduce-scatter.4
Sparse Core Ops, SparseCore 1:
  76.5 172.2 all-gather.8
  250.2 20.9 all-gather.6
  272.6 106.5 all-gather.10
